TPU v7x, 32 devices: a whole 2x2x4 slice. The times are simulated.
32 devices in a mesh: grp: 2 (over y), sp: 4 (over z), fs: 2 (over x), tp: 2 (over core).
Axes of the slice: x: 2, y: 2, z: 4, core: 2. Of those that a mesh axis runs over, the one named last changes fastest.
Arguments:
- tokens: bfloat16 [4, 2048, 2048], P(('grp', 'fs'), ('sp', 'tp')), parts along dimension 0, may hold values from -6 to 6
- norm_gain: float32 [2048], replicated, may hold values from 0.1 to 1.9
- w_bgate: bfloat16 [2048, 2048], P(('sp', 'fs'), 'tp'), may hold values from -0.125 to 0.125
- w_cgate: bfloat16 [2048, 2048], P(('sp', 'fs'), 'tp'), may hold values from -0.125 to 0.125
- w_conv_in: bfloat16 [2048, 2048], P(('sp', 'fs'), 'tp'), may hold values from -0.125 to 0.125
- conv_taps: bfloat16 [3, 2048], P(None, 'tp'), may hold values from -3.5 to 3.5
- w_query: bfloat16 [2048, 2048], P(('sp', 'fs'), 'tp'), may hold values from -0.13258252 to 0.13258252
- w_key: bfloat16 [2048, 256], P(('sp', 'fs'), 'tp'), may hold values from -4.02167 to 4.02167
- w_value: bfloat16 [2048, 256], P(('sp', 'fs'), 'tp'), may hold values from -0.125 to 0.125
- sink_logits: float32 [32], P('tp'), may hold values from 1 to 6
- conv_out_weight: bfloat16 [2048, 2048], P('tp', ('sp', 'fs')), may hold values from -0.125 to 0.125
- attn_out_weight: bfloat16 [2048, 2048], P('tp', ('sp', 'fs')), may hold values from -0.75 to 0.75
Outputs:
- mixed: bfloat16 [4, 2048, 2048], P(('grp', 'fs'), ('sp', 'tp')), parts along dimension 0
There are 2 independent parts, one for each index of `grp`. A program takes and returns all parts, laid end to end along the dimension named above; an argument that names none is the same for every part. Nothing has to cross between parts.
All inputs are finite; a program needn't handle non-finite values.
Results may differ from a plain program's by a relative error of at most 0.014.
The roundings to bfloat16 on the way count: a program that leaves them out, or rounds other values in their place, can miss the bound.
Values may be sent and summed in bfloat16 or wider, within the bound.
A program may use at most 128 MiB of HBM per device.

v0:
```python
import jax
import jax.numpy as jnp
from jax import lax
from jax.sharding import PartitionSpec as P

HEAD = 64
WINDOW = 128
TAPS = 3


epsilon = 1e-06


def shortened(array):

    def short(part):
        return part.astype(jnp.bfloat16) if part.dtype == jnp.float32 else part

    return jax.tree.map(short, array)


def shifted(array, axis, by):
    size = lax.axis_size(axis)
    pairs = [(i, i + by) for i in range(size) if 0 <= i + by < size]
    return lax.ppermute(array, axis, pairs)


def attend(queries, key_rows, value_rows, prev_keys, prev_values, sink_row, offset):
    length_here = queries.shape[0]
    kv_local = key_rows.shape[1] // HEAD
    heads_local = queries.shape[1] // HEAD
    groups = heads_local // kv_local
    blocks = length_here // WINDOW
    key_all = jnp.concatenate([prev_keys, key_rows], 0)
    value_all = jnp.concatenate([prev_values, value_rows], 0)
    key_band = jnp.concatenate(
        [
            key_all[:length_here].reshape(blocks, WINDOW, kv_local, HEAD),
            key_rows.reshape(blocks, WINDOW, kv_local, HEAD),
        ],
        1,
    )
    value_band = jnp.concatenate(
        [
            value_all[:length_here].reshape(blocks, WINDOW, kv_local, HEAD),
            value_rows.reshape(blocks, WINDOW, kv_local, HEAD),
        ],
        1,
    )
    query_blocks = queries.reshape(blocks, WINDOW, kv_local, groups, HEAD)
    scores = jnp.einsum(
        "nqhgd,nkhd->nhgqk", query_blocks, key_band, preferred_element_type=jnp.float32
    ) / jnp.sqrt(jnp.float32(HEAD))
    block_ids = jnp.arange(blocks)[:, None, None]
    query_pos = block_ids * WINDOW + jnp.arange(WINDOW)[None, :, None]
    key_pos = (block_ids - 1) * WINDOW + jnp.arange(2 * WINDOW)[None, None, :]
    allowed = (key_pos + offset >= 0) & (key_pos <= query_pos) & (query_pos - key_pos < WINDOW)
    scores = jnp.where(allowed[:, None, None], scores, -jnp.inf)
    sink_grid = sink_row.reshape(1, kv_local, groups, 1, 1)
    peak_score = jnp.maximum(jnp.max(scores, axis=-1, keepdims=True), sink_grid)
    weights = jnp.exp(scores - peak_score)
    denominator = jnp.sum(weights, axis=-1, keepdims=True) + jnp.exp(sink_grid - peak_score)
    probabilities = (weights / denominator).astype(jnp.bfloat16)
    attended = jnp.einsum(
        "nhgqk,nkhd->nqhgd", probabilities, value_band, preferred_element_type=jnp.float32
    )
    return attended.astype(jnp.bfloat16).reshape(length_here, heads_local * HEAD)


def project_all(features, weights):
    return tuple(
        (
            jnp.dot(features, weight, preferred_element_type=jnp.float32).astype(jnp.bfloat16)
            for weight in weights
        )
    )


def local(
    tokens,
    norm_gain,
    w_bgate,
    w_cgate,
    w_conv_in,
    conv_taps,
    w_query,
    w_key,
    w_value,
    sink_logits,
    conv_out_weight,
    attn_out_weight,
):
    widened = tokens[0].astype(jnp.float32)
    normed = (
        widened
        * lax.rsqrt(jnp.mean(widened * widened, axis=-1, keepdims=True) + epsilon)
        * norm_gain
    ).astype(jnp.bfloat16)
    in_weights = (w_bgate, w_cgate, w_conv_in, w_query, w_key, w_value)
    narrowed = (
        lax.all_to_all(in_weights[0], "fs", split_axis=1, concat_axis=0, tiled=True),
        lax.all_to_all(in_weights[1], "fs", split_axis=1, concat_axis=0, tiled=True),
        lax.all_to_all(in_weights[2], "fs", split_axis=1, concat_axis=0, tiled=True),
        lax.all_to_all(in_weights[3], "fs", split_axis=1, concat_axis=0, tiled=True),
        lax.all_to_all(in_weights[4], "fs", split_axis=1, concat_axis=0, tiled=True),
        lax.all_to_all(in_weights[5], "fs", split_axis=1, concat_axis=0, tiled=True),
    )
    everyone = lax.all_gather(normed, ("fs", "tp"), axis=0, tiled=True)
    whole_columns = (
        lax.all_gather(narrowed[0], "sp", axis=0, tiled=True),
        lax.all_gather(narrowed[1], "sp", axis=0, tiled=True),
        lax.all_gather(narrowed[2], "sp", axis=0, tiled=True),
        lax.all_gather(narrowed[3], "sp", axis=0, tiled=True),
        lax.all_gather(narrowed[4], "sp", axis=0, tiled=True),
        lax.all_gather(narrowed[5], "sp", axis=0, tiled=True),
    )
    rounded = project_all(everyone, whole_columns)
    projected = jax.tree.map(
        lambda part, own: part.astype(own.dtype),
        lax.all_to_all(shortened(rounded), "fs", split_axis=0, concat_axis=1, tiled=True),
        rounded,
    )
    out_gate, in_gate, conv_input, queries, key_rows, value_rows = projected
    length_here = queries.shape[0]
    gated = (in_gate.astype(jnp.float32) * conv_input.astype(jnp.float32)).astype(jnp.bfloat16)
    earlier = shifted(
        (
            gated[length_here - (TAPS - 1) :],
            key_rows[length_here - WINDOW :],
            value_rows[length_here - WINDOW :],
        ),
        "sp",
        1,
    )
    padded = jnp.concatenate([earlier[0], gated], 0)
    taps_wide = conv_taps.astype(jnp.float32)
    convolved = padded[0:length_here].astype(jnp.float32) * taps_wide[0]
    for which in range(1, TAPS):
        convolved = (
            convolved + padded[which : which + length_here].astype(jnp.float32) * taps_wide[which]
        )
    conv_branch = (out_gate.astype(jnp.float32) * convolved).astype(jnp.bfloat16)
    offset = lax.axis_index("sp") * length_here
    attended = attend(queries, key_rows, value_rows, earlier[1], earlier[2], sink_logits, offset)
    out_columns = (
        lax.all_gather(conv_out_weight, ("sp", "fs"), axis=1, tiled=True),
        lax.all_gather(attn_out_weight, ("sp", "fs"), axis=1, tiled=True),
    )
    product = jnp.dot(conv_branch, out_columns[0], preferred_element_type=jnp.float32)
    summed = lax.psum_scatter(
        (product + jnp.dot(attended, out_columns[1], preferred_element_type=jnp.float32)).astype(
            jnp.bfloat16
        ),
        "tp",
        scatter_dimension=0,
        tiled=True,
    )
    return summed[None]


def solution(mesh):
    placed = (
        P(("grp", "fs"), ("sp", "tp"), None),
        P(),
        P(("sp", "fs"), "tp"),
        P(("sp", "fs"), "tp"),
        P(("sp", "fs"), "tp"),
        P(None, "tp"),
        P(("sp", "fs"), "tp"),
        P(("sp", "fs"), "tp"),
        P(("sp", "fs"), "tp"),
        P("tp"),
        P("tp", ("sp", "fs")),
        P("tp", ("sp", "fs")),
    )
    return jax.shard_map(
        local,
        mesh=mesh,
        in_specs=placed,
        out_specs=P(("grp", "fs"), ("sp", "tp"), None),
        check_vma=False,
    )
```

profile of v0, /device:TPU:9, one launch (start us, length us, event | category | flops | bytes accessed | tf_op | source)
XLA Modules:
  0.0 432.6 jit_solution(1566950620725045063)
XLA Ops:
  6.5 1.6 fusion.3
  8.1 2.5 fusion.5
  11.0 9.7 %all_to_all.207 = bf16[256,2,512]{0,2,1:T(8,128)(2,1)S(1)} all-to-all(bf16[256,2,512]{0,2,1:T(8,128)(2,1)S(1)} %bitcast.136), channel_id=1, replica_groups=mesh['grp'=2,'sp'=4,'fs'=2,'tp'=2] {'fs'}, dimensions={1} | all-to-all | bytes 1048576 | tf_op jit(solution)/shard_map/all_to_all | solution.py:104
  20.6 1.0 copy.51
  21.9 16.1 %all_to_all.208 = bf16[256,2,512]{0,2,1:T(8,128)(2,1)S(1)} all-to-all(bf16[256,2,512]{0,2,1:T(8,128)(2,1)S(1)} %bitcast.137), channel_id=1, replica_groups=mesh['grp'=2,'sp'=4,'fs'=2,'tp'=2] {'fs'}, dimensions={1} | all-to-all | bytes 1048576 | tf_op jit(solution)/shard_map/all_to_all | solution.py:102
  38.0 1.0 copy.35
  39.4 15.9 %all_to_all.209 = bf16[256,2,512]{0,2,1:T(8,128)(2,1)S(1)} all-to-all(bf16[256,2,512]{0,2,1:T(8,128)(2,1)S(1)} %bitcast.138), channel_id=1, replica_groups=mesh['grp'=2,'sp'=4,'fs'=2,'tp'=2] {'fs'}, dimensions={1} | all-to-all | bytes 1048576 | tf_op jit(solution)/shard_map/all_to_all | solution.py:103
  55.3 1.0 copy.38
  56.6 9.0 %all_to_all.210 = bf16[256,2,512]{0,2,1:T(8,128)(2,1)S(1)} all-to-all(bf16[256,2,512]{0,2,1:T(8,128)(2,1)S(1)} %bitcast.139), channel_id=1, replica_groups=mesh['grp'=2,'sp'=4,'fs'=2,'tp'=2] {'fs'}, dimensions={1} | all-to-all | bytes 1048576 | tf_op jit(solution)/shard_map/all_to_all | solution.py:101
  65.6 1.0 copy.32
  67.2 0.7 copy.45
  68.0 3.3 all-to-all-start.8
  71.3 0.7 all-gather.20.cloned.1.call-update
  72.7 0.7 copy.40
  73.5 1.2 all-to-all-done.8
  74.6 3.3 all-to-all-start.6
  77.9 14.2 %all_gather.33 = bf16[2048,64]{0,1:T(8,128)(2,1)S(1)} all-gather(bf16[512,64]{0,1:T(8,128)(2,1)S(1)} %bitcast.150), channel_id=1, replica_groups=mesh['grp'=2,'sp'=4,'fs'=2,'tp'=2] {'sp'}, dimensions={0}, use_global_device_ids=true | all-gather | bytes 327680 | tf_op jit(solution)/shard_map/all_gather | solution.py:114
  92.2 14.8 %all_gather.32 = bf16[2048,64]{0,1:T(8,128)(2,1)S(1)} all-gather(bf16[512,64]{0,1:T(8,128)(2,1)S(1)} %bitcast.151), channel_id=1, replica_groups=mesh['grp'=2,'sp'=4,'fs'=2,'tp'=2] {'sp'}, dimensions={0}, use_global_device_ids=true | all-gather | bytes 327680 | tf_op jit(solution)/shard_map/all_gather | solution.py:115
  107.0 3.6 convolution_convert_fusion.4
  110.5 0.7 copy.78
  111.2 3.4 all-to-all-start.9
  114.6 5.3 %convolution_convert_fusion = bf16[1024,512]{1,0:T(8,128)(2,1)S(1)} fusion(bf16[1024,2048]{1,0:T(8,128)(2,1)} %all-gather.8.cloned.1.call-done, bf16[2048,512]{1,0:T(8,128)(2,1)} %all-gather.18.cloned.1.call-done), kind=kOutput, calls=%fused_computation.16 | convolution fusion | flops 2148007936 | bytes 7340032 | tf_op jit(solution)/shard_map/dot_general | solution.py:73
  120.0 1.4 convolution_convert_fusion.5
  121.4 0.7 copy.79
  122.0 3.4 all-to-all-start.7
  125.4 31.5 %all-gather.12.cloned.1.call-done = bf16[2048,512]{1,0:T(8,128)(2,1)} async-done(((bf16[512,512]{1,0:T(8,128)(2,1)}), bf16[2048,512]{1,0:T(8,128)(2,1)}) %all-gather.12.cloned.1.call-update) | async-done | bytes 2097168 | tf_op jit(solution)/shard_map/all_gather | solution.py:111
  156.9 5.2 %convolution_convert_fusion.2 = bf16[1024,512]{1,0:T(8,128)(2,1)S(1)} fusion(bf16[1024,2048]{1,0:T(8,128)(2,1)} %all-gather.8.cloned.1.call-done, bf16[2048,512]{1,0:T(8,128)(2,1)} %all-gather.12.cloned.1.call-done), kind=kOutput, calls=%fused_computation.18 | convolution fusion | flops 2148007936 | bytes 7340032 | tf_op jit(solution)/shard_map/dot_general | solution.py:73
  162.1 1.3 copy.52
  163.4 1.4 copy.36
  164.8 3.6 all-to-all-start.11
  168.4 34.3 %all-gather.14.cloned.1.call-done = bf16[2048,512]{1,0:T(8,128)(2,1)} async-done(((bf16[512,512]{1,0:T(8,128)(2,1)}), bf16[2048,512]{1,0:T(8,128)(2,1)}) %all-gather.14.cloned.1.call-update) | async-done | bytes 2097168 | tf_op jit(solution)/shard_map/all_gather | solution.py:112
  202.7 5.2 %convolution_convert_fusion.1 = bf16[1024,512]{1,0:T(8,128)(2,1)S(1)} fusion(bf16[1024,2048]{1,0:T(8,128)(2,1)} %all-gather.8.cloned.1.call-done, bf16[2048,512]{1,0:T(8,128)(2,1)} %all-gather.14.cloned.1.call-done), kind=kOutput, calls=%fused_computation.17 | convolution fusion | flops 2148007936 | bytes 7340032 | tf_op jit(solution)/shard_map/dot_general | solution.py:73
  207.9 1.3 copy.39
  209.2 3.8 all-to-all-start.3
  213.0 35.6 %all-gather.10.cloned.1.call-done = bf16[2048,512]{1,0:T(8,128)(2,1)} async-done(((bf16[512,512]{1,0:T(8,128)(2,1)}), bf16[2048,512]{1,0:T(8,128)(2,1)}) %all-gather.10.cloned.1.call-update) | async-done | bytes 2097168 | tf_op jit(solution)/shard_map/all_gather | solution.py:110
  248.6 5.2 %convolution_convert_fusion.3 = bf16[1024,512]{1,0:T(8,128)(2,1)S(1)} fusion(bf16[1024,2048]{1,0:T(8,128)(2,1)} %all-gather.8.cloned.1.call-done, bf16[2048,512]{1,0:T(8,128)(2,1)} %all-gather.10.cloned.1.call-done), kind=kOutput, calls=%fused_computation.19 | convolution fusion | flops 2148007936 | bytes 7340032 | tf_op jit(solution)/shard_map/dot_general | solution.py:73
  253.8 1.3 copy.33
  255.8 3.6 collective-permute-start.2
  260.0 2.7 collective-permute-start.1
  262.7 3.6 all-to-all-start.5
  266.3 0.7 copy_bitcast_fusion
  267.0 0.7 copy_bitcast_fusion.2
  267.6 1.4 pad_maximum_fusion.1
  269.1 0.9 reshape.180
  270.0 0.7 copy.48
  270.7 1.4 pad_maximum_fusion.2
  272.1 1.6 reshape.178
  273.7 1.6 copy.43
  275.3 1.1 reshape.182
  276.4 2.5 all-to-all-done.5
  278.9 4.4 %all-to-all-start.1 = ((bf16[2,512,512]{1,2,0:T(8,128)(2,1)}), bf16[2,512,512]{1,2,0:T(8,128)(2,1)}, u32[]{:S(2)}, u32[]{:S(2)}) async-start(bf16[2,512,512]{1,2,0:T(8,128)(2,1)} %copy.33), calls=%async_computation.1 | async-start | bytes 2097152 | tf_op jit(solution)/shard_map/all_to_all | solution.py:120
  283.8 2.3 collective-permute-start
  286.1 2.5 fusion.1
  288.8 2.4 fusion
  291.2 2.4 fusion.8
  293.6 0.9 copy.55
  294.5 5.3 %all-to-all-done.1 = bf16[2,512,512]{1,2,0:T(8,128)(2,1)} async-done(((bf16[2,512,512]{1,2,0:T(8,128)(2,1)}), bf16[2,512,512]{1,2,0:T(8,128)(2,1)}, u32[]{:S(2)}, u32[]{:S(2)}) %all-to-all-start.1) | async-done | bytes 1048608 | tf_op jit(solution)/shard_map/all_to_all | solution.py:120
  299.9 0.7 copy-done.7
  300.6 3.0 fusion.6
  303.6 29.6 %all-gather.16.cloned.1.call-done = bf16[1024,2048]{1,0:T(8,128)(2,1)} async-done(((bf16[1024,256]{1,0:T(8,128)(2,1)}), bf16[1024,2048]{1,0:T(8,128)(2,1)}) %all-gather.16.cloned.1.call-update) | async-done | bytes 4194320 | tf_op jit(solution)/shard_map/all_gather | solution.py:146
  333.2 6.6 %fusion.24 = f32[512,2048]{1,0:T(8,128)} fusion(bf16[512,1024]{0,1:T(8,128)(2,1)S(1)} %fusion.6, bf16[1024,2048]{1,0:T(8,128)(2,1)} %all-gather.16.cloned.1.call-done), kind=kOutput, calls=%fused_computation.58 | convolution fusion | flops 2147483648 | bytes 9437184 | tf_op jit(solution)/shard_map/dot_general | solution.py:149
  339.8 67.3 %all-gather.20.cloned.1.call-done = bf16[1024,2048]{1,0:T(8,128)(2,1)} async-done(((bf16[1024,256]{1,0:T(8,128)(2,1)}), bf16[1024,2048]{1,0:T(8,128)(2,1)}) %all-gather.20.cloned.1.call-update) | async-done | bytes 4194320 | tf_op jit(solution)/shard_map/all_gather | solution.py:147
  407.1 7.2 %add_convert_fusion = bf16[512,2048]{1,0:T(8,128)(2,1)} fusion(f32[512,2048]{1,0:T(8,128)} %fusion.24, bf16[1024,2048]{1,0:T(8,128)(2,1)} %all-gather.20.cloned.1.call-done, bf16[128,8,4,128]{3,2,1,0:T(4,128)(2,1)S(1)} %bitcast.127), kind=kOutput, calls=%fused_computation.5 | convolution fusion | flops 2149580800 | bytes 11534336 | tf_op jit(solution)/shard_map/dot_general | solution.py:151
  414.4 11.4 %reduce-scatter.2.cloned.1.call-done = bf16[256,2048]{1,0:T(8,128)(2,1)} async-done(((bf16[512,2048]{1,0:T(8,128)(2,1)}), bf16[256,2048]{1,0:T(8,128)(2,1)}) %reduce-scatter.2.cloned.1.call-update) | async-done | bytes 1048592 | tf_op jit(solution)/shard_map/reduce_scatter | solution.py:150
  (73 shorter events, 4.3 us)
Async XLA Ops:
  6.5 4.2 copy-start.3
  6.5 15.2 %copy-start.4 = (bf16[256,1024]{1,0:T(8,128)(2,1)S(1)}, bf16[256,1024]{1,0:T(8,128)(2,1)}, u32[]{:S(2)}) copy-start(bf16[256,1024]{1,0:T(8,128)(2,1)} %param.15) | copy-start | bytes 1572868
  6.5 100.4 %all-gather.8.cloned.1.call-start = ((), (), s32[]{:S(2)}) async-start(), calls=%async_computation.13 | async-start | bytes 5242880 | tf_op jit(solution)/shard_map/all_gather | solution.py:108
  10.7 28.5 %copy-start.5 = (bf16[256,1024]{1,0:T(8,128)(2,1)S(1)}, bf16[256,1024]{1,0:T(8,128)(2,1)}, u32[]{:S(2)}) copy-start(bf16[256,1024]{1,0:T(8,128)(2,1)} %param.16) | copy-start | bytes 1572868
  10.7 103.9 %all-gather.18.cloned.1.call-start = ((), (), s32[]{:S(2)}) async-start(), calls=%async_computation.18 | async-start | bytes 2621440 | tf_op jit(solution)/shard_map/all_gather | solution.py:113
  21.6 34.8 %copy-start.6 = (bf16[256,1024]{1,0:T(8,128)(2,1)S(1)}, bf16[256,1024]{1,0:T(8,128)(2,1)}, u32[]{:S(2)}) copy-start(bf16[256,1024]{1,0:T(8,128)(2,1)} %param.14) | copy-start | bytes 1572868
  21.7 135.2 %all-gather.12.cloned.1.call-start = ((), (), s32[]{:S(2)}) async-start(), calls=%async_computation.15 | async-start | bytes 2621440 | tf_op jit(solution)/shard_map/all_gather | solution.py:111
  39.1 28.2 %copy-start.10 = (bf16[256,128]{1,0:T(8,128)(2,1)S(1)}, bf16[256,128]{1,0:T(8,128)(2,1)}, u32[]{:S(2)}) copy-start(bf16[256,128]{1,0:T(8,128)(2,1)} %param.19) | copy-start | bytes 196612
  39.1 33.5 %copy-start.12 = (bf16[3,1024]{1,0:T(4,128)(2,1)S(1)}, bf16[3,1024]{1,0:T(4,128)(2,1)}, u32[]{:S(2)}) copy-start(bf16[3,1024]{1,0:T(4,128)(2,1)} %param.17) | copy-start | bytes 18436
  39.1 33.5 %copy-start.13 = (f32[16]{0:T(128)S(1)}, f32[16]{0:T(128)}, u32[]{:S(2)}) copy-start(f32[16]{0:T(128)} %param.21) | copy-start | bytes 196
  39.1 33.6 %copy-start.11 = (bf16[256,128]{1,0:T(8,128)(2,1)S(1)}, bf16[256,128]{1,0:T(8,128)(2,1)}, u32[]{:S(2)}) copy-start(bf16[256,128]{1,0:T(8,128)(2,1)} %param.20) | copy-start | bytes 196612
  39.1 163.6 %all-gather.14.cloned.1.call-start = ((), (), s32[]{:S(2)}) async-start(), calls=%async_computation.16 | async-start | bytes 2621440 | tf_op jit(solution)/shard_map/all_gather | solution.py:112
  56.3 192.3 %all-gather.10.cloned.1.call-start = ((), (), s32[]{:S(2)}) async-start(), calls=%async_computation.14 | async-start | bytes 2621440 | tf_op jit(solution)/shard_map/all_gather | solution.py:110
  66.6 266.6 %all-gather.16.cloned.1.call-start = ((), (), s32[]{:S(2)}) async-start(), calls=%async_computation.17 | async-start | bytes 4718592 | tf_op jit(solution)/shard_map/all_gather | solution.py:146
  68.0 6.7 %all-to-all-start.8 = ((bf16[256,2,64]{0,2,1:T(8,128)(2,1)}), bf16[256,2,64]{0,2,1:T(8,128)(2,1)S(1)}, u32[]{:S(2)}, u32[]{:S(2)}) async-start(bf16[256,2,64]{0,2,1:T(8,128)(2,1)} %bitcast.30), calls=%async_computation.8 | async-start | bytes 131072 | tf_op jit(solution)/shard_map/all_to_all | solution.py:105
  71.3 335.9 %all-gather.20.cloned.1.call-start = ((), (), s32[]{:S(2)}) async-start(), calls=%async_computation.19 | async-start | bytes 4718592 | tf_op jit(solution)/shard_map/all_gather | solution.py:147
  74.6 17.5 %all-to-all-start.6 = ((bf16[256,2,64]{0,2,1:T(8,128)(2,1)}), bf16[256,2,64]{0,2,1:T(8,128)(2,1)S(1)}, u32[]{:S(2)}, u32[]{:S(2)}) async-start(bf16[256,2,64]{0,2,1:T(8,128)(2,1)} %bitcast.23), calls=%async_computation.6 | async-start | bytes 131072 | tf_op jit(solution)/shard_map/all_to_all | solution.py:106
  111.2 10.8 %all-to-all-start.9 = ((bf16[2,512,64]{1,2,0:T(8,128)(2,1)}), bf16[2,512,64]{1,2,0:T(8,128)(2,1)S(1)}, u32[]{:S(2)}, u32[]{:S(2)}) async-start(bf16[2,512,64]{1,2,0:T(8,128)(2,1)} %bitcast.122), calls=%async_computation.9 | async-start | bytes 262144 | tf_op jit(solution)/shard_map/all_to_all | solution.py:120
  114.6 5.3 %copy-start = (bf16[1024,2048]{1,0:T(8,128)(2,1)S(1)}, bf16[1024,2048]{1,0:T(8,128)(2,1)}, u32[]{:S(2)}) copy-start(bf16[1024,2048]{1,0:T(8,128)(2,1)} %all-gather.8.cloned.1.call-done) | copy-start | bytes 12582916
  122.0 42.7 %all-to-all-start.7 = ((bf16[2,512,64]{1,2,0:T(8,128)(2,1)}), bf16[2,512,64]{1,2,0:T(8,128)(2,1)S(1)}, u32[]{:S(2)}, u32[]{:S(2)}) async-start(bf16[2,512,64]{1,2,0:T(8,128)(2,1)} %bitcast.123), calls=%async_computation.7 | async-start | bytes 262144 | tf_op jit(solution)/shard_map/all_to_all | solution.py:120
  164.8 44.5 %all-to-all-start.11 = ((bf16[2,512,512]{1,2,0:T(8,128)(2,1)}), bf16[2,512,512]{1,2,0:T(8,128)(2,1)S(1)}, u32[]{:S(2)}, u32[]{:S(2)}) async-start(bf16[2,512,512]{1,2,0:T(8,128)(2,1)} %copy.52), calls=%async_computation.11 | async-start | bytes 2097152 | tf_op jit(solution)/shard_map/all_to_all | solution.py:120
  209.2 53.4 %all-to-all-start.3 = ((bf16[2,512,512]{1,2,0:T(8,128)(2,1)}), bf16[2,512,512]{1,2,0:T(8,128)(2,1)S(1)}, u32[]{:S(2)}, u32[]{:S(2)}) async-start(bf16[2,512,512]{1,2,0:T(8,128)(2,1)} %copy.36), calls=%async_computation.3 | async-start | bytes 2097152 | tf_op jit(solution)/shard_map/all_to_all | solution.py:120
  255.8 11.9 %collective-permute-start.2 = (bf16[128,128]{0,1:T(8,128)(2,1)}, bf16[128,128]{0,1:T(8,128)(2,1)}, u32[]{:S(2)}, u32[]{:S(2)}) collective-permute-start(bf16[128,128]{0,1:T(8,128)(2,1)} %bitcast.33), channel_id=1, source_target_pairs={{0,4},{4,8},{8,12},{1,5},{5,9},{9,13},{2,6},{6,10},{10,14},{3,7},{... | collective-permute-start | bytes 98312 | tf_op jit(solution)/shard_map/ppermute | solution.py:25
  260.0 10.7 %collective-permute-start.1 = (bf16[128,128]{0,1:T(8,128)(2,1)}, bf16[128,128]{0,1:T(8,128)(2,1)}, u32[]{:S(2)}, u32[]{:S(2)}) collective-permute-start(bf16[128,128]{0,1:T(8,128)(2,1)} %bitcast.26), channel_id=1, source_target_pairs={{0,4},{4,8},{8,12},{1,5},{5,9},{9,13},{2,6},{6,10},{10,14},{3,7},{... | collective-permute-start | bytes 98312 | tf_op jit(solution)/shard_map/ppermute | solution.py:25
  262.7 16.2 %all-to-all-start.5 = ((bf16[2,512,512]{1,2,0:T(8,128)(2,1)}), bf16[2,512,512]{1,2,0:T(8,128)(2,1)S(1)}, u32[]{:S(2)}, u32[]{:S(2)}) async-start(bf16[2,512,512]{1,2,0:T(8,128)(2,1)} %copy.39), calls=%async_computation.5 | async-start | bytes 2097152 | tf_op jit(solution)/shard_map/all_to_all | solution.py:120
  272.1 14.0 %copy-start.1 = (bf16[4,128,2,64]{1,3,2,0:T(8,128)(2,1)S(1)}, bf16[4,128,2,64]{1,3,2,0:T(8,128)(2,1)}, u32[]{:S(2)}) copy-start(bf16[4,128,2,64]{1,3,2,0:T(8,128)(2,1)} %copy_bitcast_fusion) | copy-start | bytes 393220
  272.1 14.0 %copy-start.2 = (bf16[4,128,2,64]{1,3,2,0:T(8,128)(2,1)S(1)}, bf16[4,128,2,64]{1,3,2,0:T(8,128)(2,1)}, u32[]{:S(2)}) copy-start(bf16[4,128,2,64]{1,3,2,0:T(8,128)(2,1)} %copy.48) | copy-start | bytes 393220
  278.9 21.0 %all-to-all-start.1 = ((bf16[2,512,512]{1,2,0:T(8,128)(2,1)}), bf16[2,512,512]{1,2,0:T(8,128)(2,1)}, u32[]{:S(2)}, u32[]{:S(2)}) async-start(bf16[2,512,512]{1,2,0:T(8,128)(2,1)} %copy.33), calls=%async_computation.1 | async-start | bytes 2097152 | tf_op jit(solution)/shard_map/all_to_all | solution.py:120
  283.3 142.4 %reduce-scatter.2.cloned.1.call-start = ((), (), s32[]{:S(2)}) async-start(), calls=%async_computation.20 | async-start | bytes 3145728 | tf_op jit(solution)/shard_map/reduce_scatter | solution.py:150
  283.8 16.1 %collective-permute-start = (bf16[2,1024]{0,1:T(8,128)(2,1)S(1)}, bf16[2,1024]{0,1:T(8,128)(2,1)S(1)}, u32[]{:S(2)}, u32[]{:S(2)}) collective-permute-start(bf16[2,1024]{0,1:T(8,128)(2,1)S(1)} %bitcast.152), channel_id=1, source_target_pairs={{0,4},{4,8},{8,12},{1,5},{5,9},{9,13},{2,6},{6,10},{10,14},{3,7},{... | collective-permute-start | bytes 12296 | tf_op jit(solution)/shard_map/ppermute | solution.py:25
  288.8 2.5 copy-start.8
  288.8 2.5 copy-start.9
  299.9 0.7 copy-start.7
Sparse Core Ops, SparseCore 0:
  10.8 46.6 all-gather.7
  59.1 51.1 all-gather.17
  111.9 44.9 all-gather.11
  158.3 44.3 all-gather.13
  204.1 44.4 all-gather.9
  250.5 82.6 all-gather.15
  335.2 71.8 all-gather.19
  414.5 11.2 reduce-scatter.1
where the time goes:
time: 435 us; the launch traced here: 433 us
  waiting for transfers between devices  220 us (51%)
  blocking collectives  79.7 us (18%)
  matrix products  44.6 us (10%)
  starting transfers between devices  37.6 us (9%)
  local copies, waits for them, and re-layouts  23.4 us (5%)
  between operations  13.9 us (3%)
  other arithmetic  13.3 us (3%)
    all_gather x1, waiting for transfers between devices, local(): lax.all_gather(attn_out_weight, ('sp', 'fs'), axis=1, tiled=True)  67.3 us
    all_gather x1, waiting for transfers between devices, local(): lax.all_gather(narrowed[0], 'sp', axis=0, tiled=True)  35.6 us
    all_gather x1, waiting for transfers between devices, local(): lax.all_gather(narrowed[2], 'sp', axis=0, tiled=True)  34.3 us
    all_gather x1, waiting for transfers between devices, local(): lax.all_gather(narrowed[1], 'sp', axis=0, tiled=True)  31.5 us
    all_gather x1, waiting for transfers between devices, local(): lax.all_gather(conv_out_weight, ('sp', 'fs'), axis=1, tiled=True)  29.6 us
    dot_general x6, matrix products, project_all(): jnp.dot(features, weight, preferred_element_type=jnp.float32)  25.9 us
    all_to_all x6, starting transfers between devices, local(): lax.all_to_all(shortened(rounded), 'fs', split_axis=0, concat_axis=1, til...  22.2 us
    all_to_all x1, blocking collectives, local(): lax.all_to_all(in_weights[1], 'fs', split_axis=1, concat_axis=0, tiled=True)  16.1 us
  transfers between devices with their start and end apart: 19, of which 9 were waited for; matrix products, arithmetic and copies ran while one was open for 16% of the time, Pallas kernels for 0%

commit v1 on v0

v1 whole, which is shorter than its diff:
```python
import functools

import jax
import jax.numpy as jnp
from jax import lax
from jax.experimental import pallas as pl
from jax.experimental.pallas import tpu as pltpu
from jax.sharding import PartitionSpec as P

HEAD = 64
WINDOW = 128
TAPS = 3
LANES = 128
HALO = 16
TILE = 256
MESH = pl.DeviceIdType.MESH

epsilon = 1e-06


def spans(kv, conv):
    third = conv * 3 // 8 // LANES * LANES
    arrays = [(0, 2 * kv, kv)]
    for which in range(6):
        arrays.append((2 * kv + which * conv, conv, third))
    return arrays


def kernel(
    sizes,
    normed,
    packed,
    taps,
    sink,
    out,
    weights,
    rows,
    query,
    keys,
    gate,
    gated,
    conv,
    attended,
    partial,
    theirs,
    local_sem,
    pair_sem,
    halo_sem,
    z_send,
    x_send,
    y_send,
    zx_recv,
    y_recv,
    swap_send,
    swap_recv,
):
    n, m, own, kv, width = sizes
    depth = weights.shape[1]
    features = rows.shape[1]
    length = 2 * own
    grp, sp = lax.axis_index("grp"), lax.axis_index("sp")
    fs, tp = lax.axis_index("fs"), lax.axis_index("tp")
    arrays = spans(kv, width)
    mine = sp * m + fs

    barrier = pltpu.get_barrier_semaphore()

    def greet(axis, device):
        pl.semaphore_signal(barrier, inc=1, device_id={axis: device}, device_id_type=MESH)

    fill = pltpu.make_async_copy(packed, weights.at[mine], local_sem.at[0])
    fill.start()
    at_own = pl.multiple_of(WINDOW + tp * own, LANES)
    place = pltpu.make_async_copy(normed, rows.at[pl.ds(at_own, own)], local_sem.at[1])
    place.start()

    def greet_sp(d, _):
        greet("sp", lax.rem(sp + d, n))
        return _

    def greet_fs(d, _):
        greet("fs", lax.rem(fs + d, m))
        return _

    lax.fori_loop(1, n, greet_sp, 0)
    lax.fori_loop(1, m, greet_fs, 0)
    greet("grp", 1 - grp)
    greet("tp", 1 - tp)
    pl.semaphore_wait(barrier, n + m)

    sibling = pltpu.make_async_remote_copy(
        normed,
        rows.at[pl.ds(at_own, own)],
        pair_sem.at[0],
        pair_sem.at[1],
        device_id={"tp": 1 - tp},
        device_id_type=MESH,
    )
    sibling.start()

    def halo_copy(source, where):
        return pltpu.make_async_remote_copy(
            source,
            rows.at[pl.ds(0, WINDOW)],
            halo_sem.at[0],
            halo_sem.at[1],
            device_id=where,
            device_id_type=MESH,
        )

    onward = halo_copy(normed.at[pl.ds(own - WINDOW, WINDOW)], {"sp": lax.rem(sp + 1, n)})
    across = pltpu.make_async_remote_copy(
        rows.at[pl.ds(0, WINDOW)],
        rows.at[pl.ds(0, WINDOW)],
        halo_sem.at[2],
        halo_sem.at[1],
        device_id={"tp": 1 - tp},
        device_id_type=MESH,
    )

    @pl.when((tp == 1) & (sp < n - 1))
    def _():
        onward.start()

    @pl.when(sp == 0)
    def _():
        rows[pl.ds(0, WINDOW), :] = jnp.zeros((WINDOW, features), jnp.bfloat16)

    fill.wait()

    def fetched(j):
        first, total, alone = arrays[j]
        return pl.ds(pl.multiple_of(first + grp * alone, LANES), total - alone)

    def lone(j, group):
        first, total, alone = arrays[j]
        return pl.ds(pl.multiple_of(first + group * (total - alone), LANES), alone)

    def along_z(j, d, chunk):
        piece = weights.at[chunk, :, fetched(j)]
        return pltpu.make_async_remote_copy(
            piece,
            piece,
            z_send.at[j, d],
            zx_recv.at[j, chunk],
            device_id={"sp": lax.rem(sp + d, n)},
            device_id_type=MESH,
        )

    def along_x(j, s, d, chunk):
        piece = weights.at[chunk, :, fetched(j)]
        return pltpu.make_async_remote_copy(
            piece,
            piece,
            x_send.at[j, s, d],
            zx_recv.at[j, chunk],
            device_id={"fs": lax.rem(fs + d, m)},
            device_id_type=MESH,
        )

    def along_y(j, chunk, group):
        piece = weights.at[chunk, :, lone(j, group)]
        return pltpu.make_async_remote_copy(
            piece,
            piece,
            y_send.at[j, chunk],
            y_recv.at[j, chunk],
            device_id={"grp": 1 - grp},
            device_id_type=MESH,
        )

    def loop(low, high, body):
        def step(i, carry):
            body(i)
            return carry

        lax.fori_loop(low, high, step, 0)

    def open_links(j):
        loop(1, n, lambda d: along_z(j, d, mine).start())
        loop(1, m, lambda d: along_x(j, sp, d, mine).start())

    def from_z(j):
        def body(d):
            s = lax.rem(sp + d, n)
            chunk = s * m + fs
            along_z(j, d, chunk).wait_recv()
            loop(1, m, lambda e: along_x(j, s, e, chunk).start())
            along_y(j, chunk, grp).start()

        loop(1, n, body)

    def from_x(j):
        def body(d):
            s = lax.rem(sp + d, n)

            def inner(e):
                chunk = s * m + lax.rem(fs + e, m)
                along_x(j, s, e, chunk).wait_recv()
                along_y(j, chunk, grp).start()

            loop(1, m, inner)

        loop(0, n, body)

    def from_y(j):
        def body(d):
            chunk = lax.rem(mine + d, n * m)
            along_y(j, chunk, 1 - grp).wait_recv()

        loop(1, n * m, body)

    for j in range(len(arrays)):
        open_links(j)

    place.wait()
    sibling.wait()

    @pl.when((tp == 1) & (sp > 0))
    def _():
        onward.wait_recv()
        across.start()

    @pl.when((tp == 0) & (sp > 0))
    def _():
        across.wait_recv()

    def project(first, low, count, columns):
        block = weights[:, :, pl.ds(first, columns)].reshape(n * m * depth, columns)
        return jnp.dot(
            rows[pl.ds(low, count), :], block, preferred_element_type=jnp.float32
        ).astype(jnp.bfloat16)

    def tiles(total, body):
        step = min(TILE, total)
        loop(0, total // step, lambda t: body(pl.multiple_of(t * step, LANES), step))

    def do_keys():
        keys[...] = project(0, 0, WINDOW + length, 2 * kv)

    def do_query():
        def body(at, step):
            query[:, pl.ds(at, step)] = project(arrays[1][0] + at, WINDOW, length, step)

        tiles(width, body)

    def do_attention():
        pairs = 2 * HEAD
        per_kv = width // kv
        blocks = length // WINDOW
        place_q = lax.broadcasted_iota(jnp.int32, (WINDOW, 2 * WINDOW), 0)
        place_k = lax.broadcasted_iota(jnp.int32, (WINDOW, 2 * WINDOW), 1)
        banded = (place_k > place_q) & (place_k <= place_q + WINDOW)
        for head in range(kv // HEAD):

            def body(i):
                b = i // (per_kv // 2)
                p = lax.rem(i, per_kv // 2)
                at = pl.multiple_of((head * (per_kv // 2) + p) * pairs, LANES)
                row = pl.multiple_of(b * WINDOW, WINDOW)
                band = keys[pl.ds(row, 2 * WINDOW), :]
                key = band[:, head * HEAD : (head + 1) * HEAD]
                value = band[:, kv + head * HEAD : kv + (head + 1) * HEAD]
                least = jnp.where((sp == 0) & (b == 0), WINDOW, 0)
                allowed = banded & (place_k >= least)
                both = query[pl.ds(row, WINDOW), pl.ds(at, pairs)]
                results = []
                for half in range(2):
                    one = both[:, half * HEAD : (half + 1) * HEAD]
                    scores = lax.dot_general(
                        one, key, (((1,), (1,)), ((), ())), preferred_element_type=jnp.float32
                    ) * (1.0 / HEAD**0.5)
                    scores = jnp.where(allowed, scores, -jnp.inf)
                    logit = sink[head * per_kv + 2 * p + half]
                    peak = jnp.maximum(jnp.max(scores, axis=-1, keepdims=True), logit)
                    powers = jnp.exp(scores - peak)
                    total = jnp.sum(powers, axis=-1, keepdims=True) + jnp.exp(logit - peak)
                    probs = (powers / total).astype(jnp.bfloat16)
                    results.append(jnp.dot(probs, value, preferred_element_type=jnp.float32))
                attended[pl.ds(row, WINDOW), pl.ds(at, pairs)] = jnp.concatenate(
                    results, axis=1
                ).astype(jnp.bfloat16)

            loop(0, blocks * (per_kv // 2), body)

    def do_gate():
        def body(at, step):
            gate[:, pl.ds(at, step)] = project(
                arrays[2][0] + at, WINDOW - HALO, HALO + length, step
            )

        tiles(width, body)

    def do_gated():
        def body(at, step):
            values = project(arrays[3][0] + at, WINDOW - HALO, HALO + length, step)
            product = gate[:, pl.ds(at, step)].astype(jnp.float32) * values.astype(jnp.float32)
            gated[:, pl.ds(at, step)] = product.astype(jnp.bfloat16).astype(jnp.float32)

        tiles(width, body)

    def do_conv():
        def body(at, step):
            outer = project(arrays[4][0] + at, WINDOW, length, step).astype(jnp.float32)
            mixed = None
            for which in range(TAPS):
                tap = taps[pl.ds(which, 1), pl.ds(at, step)].astype(jnp.float32)
                term = tap * gated[pl.ds(HALO - TAPS + 1 + which, length), pl.ds(at, step)]
                mixed = term if mixed is None else mixed + term
            conv[:, pl.ds(at, step)] = (outer * mixed).astype(jnp.bfloat16)

        tiles(width, body)

    work = [do_keys, do_query, do_gate, do_gated, do_conv, None, None]
    count = len(arrays)
    for step in range(count + 2):
        if step < count:
            from_z(step)
        if 0 <= step - 1 < count:
            from_x(step - 1)
        if step >= 2:
            from_y(step - 2)
            if work[step - 2] is not None:
                work[step - 2]()
            if step == 4:
                do_attention()

    def swap(t, step):
        piece = pl.ds(pl.multiple_of(t * step, LANES), step)
        return pltpu.make_async_remote_copy(
            partial.at[1, :, piece],
            theirs.at[:, piece],
            swap_send.at[t],
            swap_recv.at[t],
            device_id={"tp": 1 - tp},
            device_id_type=MESH,
        )

    step = depth
    per = max(1, TILE // depth)
    step = per * depth
    count_out = n * m // per

    def share(low, t):
        total = None
        for j, left in ((5, conv), (6, attended)):
            block = weights[pl.ds(t * per, per), :, pl.ds(arrays[j][0], width)]
            term = lax.dot_general(
                left[pl.ds(low, own), :],
                block.reshape(step, width),
                (((1,), (1,)), ((), ())),
                preferred_element_type=jnp.float32,
            )
            total = term if total is None else total + term
        return total.astype(jnp.bfloat16)

    def final(t):
        piece = pl.ds(pl.multiple_of(t * step, LANES), step)
        partial[1, :, piece] = share(pl.multiple_of((1 - tp) * own, LANES), t)
        partial[0, :, piece] = share(pl.multiple_of(tp * own, LANES), t)
        swap(t, step).start()

    loop(0, count_out, final)

    def add(t):
        piece = pl.ds(pl.multiple_of(t * step, LANES), step)
        swap(t, step).wait()
        out[:, piece] = (
            partial[0, :, piece].astype(jnp.float32) + theirs[:, piece].astype(jnp.float32)
        ).astype(jnp.bfloat16)

    loop(0, count_out, add)

    for j in range(count):
        loop(1, n, lambda d: along_z(j, d, mine).wait_send())

        def x_done(d):
            s = lax.rem(sp + d, n)
            loop(1, m, lambda e: along_x(j, s, e, s * m + fs).wait_send())

        loop(0, n, x_done)
        loop(1, n * m, lambda d: along_y(j, lax.rem(mine + d, n * m), grp).wait_send())

    @pl.when((tp == 1) & (sp < n - 1))
    def _():
        onward.wait_send()

    @pl.when((tp == 1) & (sp > 0))
    def _():
        across.wait_send()


def local(
    n,
    m,
    tokens,
    norm_gain,
    w_bgate,
    w_cgate,
    w_conv_in,
    conv_taps,
    w_query,
    w_key,
    w_value,
    sink_logits,
    conv_out_weight,
    attn_out_weight,
):
    widened = tokens[0].astype(jnp.float32)
    normed = (
        widened
        * lax.rsqrt(jnp.mean(widened * widened, axis=-1, keepdims=True) + epsilon)
        * norm_gain
    ).astype(jnp.bfloat16)
    packed = jnp.concatenate(
        [
            w_key,
            w_value,
            w_query,
            w_cgate,
            w_conv_in,
            w_bgate,
            conv_out_weight.T,
            attn_out_weight.T,
        ],
        1,
    )
    own, features = normed.shape
    length = 2 * own
    kv, width = w_key.shape[1], w_query.shape[1]
    depth = packed.shape[0]
    arrays = len(spans(kv, width))
    chunks = n * m
    bf16 = jnp.bfloat16
    vmem = pl.BlockSpec(memory_space=pltpu.VMEM)
    whole = pl.BlockSpec(memory_space=pl.ANY)
    dma = pltpu.SemaphoreType.DMA
    mixed = pl.pallas_call(
        functools.partial(kernel, (n, m, own, kv, width)),
        out_shape=jax.ShapeDtypeStruct((own, features), bf16),
        in_specs=[whole, whole, vmem, pl.BlockSpec(memory_space=pltpu.SMEM)],
        out_specs=vmem,
        scratch_shapes=[
            pltpu.VMEM((chunks,) + packed.shape, bf16),
            pltpu.VMEM((WINDOW + length, features), bf16),
            pltpu.VMEM((length, width), bf16),
            pltpu.VMEM((WINDOW + length, 2 * kv), bf16),
            pltpu.VMEM((HALO + length, width), bf16),
            pltpu.VMEM((HALO + length, width), jnp.float32),
            pltpu.VMEM((length, width), bf16),
            pltpu.VMEM((length, width), bf16),
            pltpu.VMEM((2, own, features), bf16),
            pltpu.VMEM((own, features), bf16),
            dma((2,)),
            dma((2,)),
            dma((3,)),
            dma((arrays, n)),
            dma((arrays, n, m)),
            dma((arrays, chunks)),
            dma((arrays, chunks)),
            dma((arrays, chunks)),
            dma((chunks,)),
            dma((chunks,)),
        ],
        compiler_params=pltpu.CompilerParams(
            collective_id=0, has_side_effects=True, vmem_limit_bytes=64_000_000
        ),
    )(normed, packed, conv_taps, sink_logits)
    return mixed[None]


def solution(mesh):
    placed = (
        P(("grp", "fs"), ("sp", "tp"), None),
        P(),
        P(("sp", "fs"), "tp"),
        P(("sp", "fs"), "tp"),
        P(("sp", "fs"), "tp"),
        P(None, "tp"),
        P(("sp", "fs"), "tp"),
        P(("sp", "fs"), "tp"),
        P(("sp", "fs"), "tp"),
        P("tp"),
        P("tp", ("sp", "fs")),
        P("tp", ("sp", "fs")),
    )
    return jax.shard_map(
        functools.partial(local, mesh.shape["sp"], mesh.shape["fs"]),
        mesh=mesh,
        in_specs=placed,
        out_specs=P(("grp", "fs"), ("sp", "tp"), None),
        check_vma=False,
    )
```

time: 435 us -> 304 us (0.70)
  Pallas kernels: 0 us -> 288 us
  waiting for transfers between devices: 220 us -> 0 us
  blocking collectives: 79.7 us -> 0 us
  matrix products: 44.6 us -> 0 us
  starting transfers between devices: 37.6 us -> 0 us
  between operations: 13.9 us -> 0.04 us
  other arithmetic: 13.3 us -> 1.57 us
  local copies, waits for them, and re-layouts: 23.4 us -> 14.2 us
    pallas_call x0 -> x1, Pallas kernels: none -> 288 us  [local(): pl.pallas_call(functools.partial(kernel, (n, m, own, kv, width)), out_sha...]
    all_gather x7 -> x0, waiting for transfers between devices: 198 us -> none  [the longest x1 67.3 us: local(): lax.all_gather(attn_out_weight, ('sp', 'fs'), axis=1, tiled=True)]
    all_to_all x4 -> x0, blocking collectives: 50.7 us -> none  [the longest x1 16.1 us: local(): lax.all_to_all(in_weights[1], 'fs', split_axis=1, concat_axis=0, tiled=True)]
    dot_general x10 -> x0, matrix products: 44.6 us -> none  [the longest x6 25.9 us: project_all(): jnp.dot(features, weight, preferred_element_type=jnp.float32)]
    all_gather x2 -> x0, blocking collectives: 29 us -> none  [the longest x1 14.8 us: local(): lax.all_gather(narrowed[5], 'sp', axis=0, tiled=True)]
    all_to_all x8 -> x0, starting transfers between devices: 28.8 us -> none  [the longest x6 22.2 us: local(): lax.all_to_all(shortened(rounded), 'fs', split_axis=0, concat_axis=1, til...]
    reduce_scatter x1 -> x0, waiting for transfers between devices: 11.4 us -> none  [local(): lax.psum_scatter((product + jnp.dot(attended, out_columns[1], preferred_e...]
    all_to_all x12 -> x0, local copies, waits for them, and re-layouts: 10.8 us -> none  [the longest x6 6.7 us: local(): lax.all_to_all(shortened(rounded), 'fs', split_axis=0, concat_axis=1, til...]
  transfers between devices with their start and end apart: 19 -> 0, of which waited for: 9 -> 0; matrix products, arithmetic and copies ran while one was open for 16% -> 0% of each run, Pallas kernels for 0% -> 0%
where the time goes in v1:
time: 304 us
  Pallas kernels  288 us (95%)
  local copies, waits for them, and re-layouts  14.2 us (5%)
    pallas_call x1, Pallas kernels, local(): pl.pallas_call(functools.partial(kernel, (n, m, own, kv, width)), out_sha...  288 us
    unnamed x20, local copies, waits for them, and re-layouts  13.4 us

profile of v1, /device:TPU:9, one launch (start us, length us, event | category | flops | bytes accessed | tf_op | source)
XLA Modules:
  0.0 303.7 jit_solution(3968608098938735323)
XLA Ops:
  0.0 0.0 copy-start.1
  0.0 0.0 copy-start.2
  0.0 0.0 copy-start.3
  0.0 1.6 constant_dynamic-update-slice_fusion.5
  1.6 1.5 constant_dynamic-update-slice_fusion.4
  3.1 2.0 constant_dynamic-update-slice_fusion.3
  5.1 1.9 constant_dynamic-update-slice_fusion.2
  6.9 0.0 copy-start
  6.9 2.0 constant_dynamic-update-slice_fusion.1
  8.9 0.0 copy-done.1
  8.9 0.0 copy-start.4
  8.9 0.8 constant_dynamic-update-slice_fusion
  9.8 0.0 copy-done.2
  9.8 0.2 copy.13
  10.0 0.9 bitcast_dynamic-update-slice_fusion.1
  10.9 0.0 copy-done.3
  10.9 0.2 copy.14
  11.1 0.9 bitcast_dynamic-update-slice_fusion.packed
  11.9 0.0 copy-done
  11.9 0.3 fusion
  12.2 0.0 copy-done.4
  12.2 1.3 fusion.2.normed
  13.5 287.9 %shard_map.118 = bf16[256,2048]{1,0:T(8,128)(2,1)} custom-call(bf16[256,2048]{1,0:T(8,128)(2,1)} %fusion.2.normed, bf16[256,6400]{1,0:T(8,128)(2,1)} %bitcast_dynamic-update-slice_fusion.packed, bf16[3,1024]{1,0:T(4,128)(2,1)} %taps.1, f32[16]{0:T(128)} %sink.1), custom_call_target="tpu_custom_call" | custom-call | tf_op jit(solution)/shard_map/pallas_call | solution.py:438
  301.4 2.3 copy.23
  (1 shorter events, 0.0 us)
Async XLA Ops:
  0.0 8.9 %copy-start.1 = (bf16[256,1024]{1,0:T(8,128)(2,1)S(1)}, bf16[256,1024]{1,0:T(8,128)(2,1)}, u32[]{:S(2)}) copy-start(bf16[256,1024]{1,0:T(8,128)(2,1)} %param.14) | copy-start | bytes 1572868
  0.0 9.8 %copy-start.2 = (bf16[1024,256]{1,0:T(8,128)(2,1)S(1)}, bf16[1024,256]{1,0:T(8,128)(2,1)}, u32[]{:S(2)}) copy-start(bf16[1024,256]{1,0:T(8,128)(2,1)} %param.22) | copy-start | bytes 1572868
  0.0 10.8 %copy-start.3 = (bf16[1024,256]{1,0:T(8,128)(2,1)S(1)}, bf16[1024,256]{1,0:T(8,128)(2,1)}, u32[]{:S(2)}) copy-start(bf16[1024,256]{1,0:T(8,128)(2,1)} %param.23) | copy-start | bytes 1572868
  6.9 5.0 %copy-start = (bf16[1,256,2048]{2,1,0:T(8,128)(2,1)S(1)}, bf16[1,256,2048]{2,1,0:T(8,128)(2,1)}, u32[]{:S(2)}) copy-start(bf16[1,256,2048]{2,1,0:T(8,128)(2,1)} %param.12) | copy-start | bytes 3145732
  8.9 3.3 %copy-start.4 = (f32[2048]{0:T(1024)S(1)}, f32[2048]{0:T(1024)}, u32[]{:S(2)}) copy-start(f32[2048]{0:T(1024)} %param.13) | copy-start | bytes 24580

commit v2 on v0

v2 whole, which is shorter than its diff:
```python
import functools

import jax
import jax.numpy as jnp
from jax import lax
from jax.experimental import pallas as pl
from jax.experimental.pallas import tpu as pltpu
from jax.sharding import PartitionSpec as P

HEAD = 64
WINDOW = 128
TAPS = 3
LANES = 128
HALO = 16
TILE = 256
UNIT = 16
MESH = pl.DeviceIdType.MESH

epsilon = 1e-06


def part(count, eighths):
    return max(UNIT, count * eighths // 8 // UNIT * UNIT)


def kernel(
    n,
    m,
    normed,
    w_key,
    w_value,
    w_query,
    w_cgate,
    w_conv_in,
    w_bgate,
    conv_weight,
    attn_weight,
    taps,
    sink,
    out,
    w_in,
    w_out,
    rows,
    query,
    keys,
    gate,
    mine_conv,
    conv,
    attended,
    total,
    partial,
    theirs,
    local_sem,
    rows_send,
    rows_recv,
    halo_send,
    halo_recv,
    trade_send,
    trade_recv,
    in_send,
    in_recv,
    in_y_send,
    in_y_recv,
    z_send,
    x_send,
    out_recv,
    y_send,
    y_recv,
    give_send,
    give_recv,
    swap_send,
    swap_recv,
):
    inputs = (w_key, w_value, w_query, w_cgate, w_conv_in, w_bgate)
    outputs = (conv_weight, attn_weight)
    own, features = normed.shape
    length = 2 * own
    span = WINDOW + length
    depth, kv = w_key.shape
    width = w_query.shape[1]
    slim = width // m
    across_out = conv_weight.shape[1]
    heads = slim // HEAD
    per_kv = width // kv
    chunks = n * m
    firsts = [0, kv] + [2 * kv + i * slim for i in range(4)]
    sizes = [kv, kv] + [slim] * 4
    in_alone = [part(depth, 4)] * 6
    out_alone = [part(width, 4), part(width, 3)]

    grp, sp = lax.axis_index("grp"), lax.axis_index("sp")
    fs, tp = lax.axis_index("fs"), lax.axis_index("tp")
    mine = sp * m + fs

    def loop(low, high, body):
        def step(i, carry):
            body(i)
            return carry

        lax.fori_loop(low, high, step, 0)

    def remote(source, target, send, recv, where):
        return pltpu.make_async_remote_copy(
            source, target, send, recv, device_id=where, device_id_type=MESH
        )

    def to_sp(d):
        return {"sp": lax.rem(sp + d, n)}

    def to_fs(e):
        return {"fs": lax.rem(fs + e, m)}

    other_core = {"tp": 1 - tp}
    other_grp = {"grp": 1 - grp}

    def columns(j, f):
        if j < 2:
            return pl.ds(0, kv)
        return pl.ds(pl.multiple_of(f * slim, LANES), slim)

    def kept(j):
        return pl.ds(firsts[j], sizes[j])

    fills = [
        pltpu.make_async_copy(
            inputs[j].at[:, columns(j, fs)], w_in.at[mine, :, kept(j)], local_sem.at[j]
        )
        for j in range(6)
    ] + [
        pltpu.make_async_copy(outputs[j], w_out.at[j, mine], local_sem.at[6 + j]) for j in range(2)
    ]
    at_own = pl.multiple_of(WINDOW + tp * own, LANES)
    at_other = pl.multiple_of(WINDOW + (1 - tp) * own, LANES)
    fills.append(
        pltpu.make_async_copy(normed, rows.at[fs, pl.ds(at_own, own)], local_sem.at[8])
    )
    for fill in fills:
        fill.start()

    @pl.when(sp == 0)
    def _():
        for i in range(m):
            rows[i, pl.ds(0, WINDOW), :] = jnp.zeros((WINDOW, features), jnp.bfloat16)

    barrier = pltpu.get_barrier_semaphore()

    def greet(where):
        pl.semaphore_signal(barrier, inc=1, device_id=where, device_id_type=MESH)

    loop(1, n, lambda d: greet(to_sp(d)))
    loop(1, m, lambda e: greet(to_fs(e)))
    greet(other_grp)
    greet(other_core)
    pl.semaphore_wait(barrier, n + m)

    def trade(j, e):
        f = lax.rem(fs + e, m)
        return remote(
            inputs[j].at[:, columns(j, f)],
            w_in.at[mine, :, kept(j)],
            trade_send.at[j, e],
            trade_recv.at[j, fs],
            {"fs": f},
        )

    def trade_arrival(j, f):
        piece = w_in.at[sp * m + f, :, kept(j)]
        return remote(piece, piece, trade_send.at[j, 0], trade_recv.at[j, f], to_fs(1))

    def in_rows(j):
        return pl.ds(pl.multiple_of(grp * in_alone[j], UNIT), depth - in_alone[j])

    def in_lone(j, group):
        return pl.ds(
            pl.multiple_of(group * (depth - in_alone[j]), UNIT), in_alone[j]
        )

    def in_z(j, d, chunk, f):
        piece = w_in.at[chunk, in_rows(j), kept(j)]
        return remote(piece, piece, in_send.at[j, d, f], in_recv.at[j, chunk], to_sp(d))

    def in_y(j, chunk, group):
        piece = w_in.at[chunk, in_lone(j, group), kept(j)]
        return remote(piece, piece, in_y_send.at[j, chunk], in_y_recv.at[j, chunk], other_grp)

    def rows_copy(source, f, core, send, where):
        at = pl.multiple_of(WINDOW + core * own, LANES)
        return remote(
            source, rows.at[f, pl.ds(at, own)], rows_send.at[send], rows_recv.at[f, core], where
        )

    def rows_x(e):
        return rows_copy(normed, fs, tp, e, to_fs(e))

    def rows_core(f):
        return rows_copy(rows.at[f, pl.ds(at_own, own)], f, tp, m + f, other_core)

    def halo_copy(source, f, send, where):
        return remote(
            source, rows.at[f, pl.ds(0, WINDOW)], halo_send.at[send], halo_recv.at[f], where
        )

    def halo_here(f):
        return rows.at[f, pl.ds(0, WINDOW)]

    onward = halo_copy(normed.at[pl.ds(own - WINDOW, WINDOW)], fs, 0, to_sp(1))

    def out_rows(j):
        return pl.ds(pl.multiple_of(grp * out_alone[j], UNIT), width - out_alone[j])

    def out_lone(j, group):
        return pl.ds(pl.multiple_of(group * (width - out_alone[j]), UNIT), out_alone[j])

    def along_z(j, d):
        piece = w_out.at[j, mine, out_rows(j)]
        return remote(piece, piece, z_send.at[j, d], out_recv.at[j, mine], to_sp(d))

    def along_x(j, s, e, chunk):
        piece = w_out.at[j, chunk, out_rows(j)]
        return remote(piece, piece, x_send.at[j, s, e], out_recv.at[j, chunk], to_fs(e))

    def arrival(j, chunk):
        piece = w_out.at[j, chunk, out_rows(j)]
        return remote(piece, piece, z_send.at[j, 0], out_recv.at[j, chunk], to_sp(1))

    def along_y(j, chunk, group):
        piece = w_out.at[j, chunk, out_lone(j, group)]
        return remote(piece, piece, y_send.at[j, chunk], y_recv.at[j, chunk], other_grp)

    for j in range(6):
        loop(1, m, lambda e: trade(j, e).start())
        if j == 1:

            @pl.when((tp == 1) & (sp < n - 1))
            def _():
                onward.start()

    loop(1, m, lambda e: rows_x(e).start())
    for j in range(6):
        fills[j].wait()
        loop(1, n, lambda d: in_z(j, d, mine, fs).start())
    fills[8].wait()
    rows_core(fs).start()
    for j in range(6):

        def traded(e):
            f = lax.rem(fs + e, m)
            trade_arrival(j, f).wait_recv()
            loop(1, n, lambda d: in_z(j, d, sp * m + f, f).start())

        loop(1, m, traded)
    for j in range(2):
        fills[6 + j].wait()
        loop(1, n, lambda d: along_z(j, d).start())
        loop(1, m, lambda e: along_x(j, sp, e, mine).start())

    def rows_on(e):
        f = lax.rem(fs + e, m)
        rows_copy(rows.at[f, pl.ds(at_own, own)], f, tp, 0, to_fs(e)).wait_recv()
        rows_core(f).start()

    loop(1, m, rows_on)

    @pl.when((tp == 1) & (sp > 0))
    def _():
        halo_copy(halo_here(fs), fs, 0, other_core).wait_recv()
        halo_copy(halo_here(fs), fs, 1 + fs, other_core).start()
        loop(1, m, lambda e: halo_copy(halo_here(fs), fs, m + e, to_fs(e)).start())

        def pass_on(e):
            f = lax.rem(fs + e, m)
            halo_copy(halo_here(f), f, 0, other_core).wait_recv()
            halo_copy(halo_here(f), f, 1 + f, other_core).start()

        loop(1, m, pass_on)

    def rows_in(f):
        piece = rows.at[f, pl.ds(at_other, own)]
        remote(piece, piece, rows_send.at[0], rows_recv.at[f, 1 - tp], other_core).wait_recv()

    loop(0, m, rows_in)

    @pl.when((tp == 0) & (sp > 0))
    def _():
        loop(0, m, lambda f: halo_copy(halo_here(f), f, 0, other_core).wait_recv())

    def in_from_z(j):
        def body(i):
            s = lax.rem(sp + 1 + i // m, n)
            chunk = s * m + lax.rem(fs + i, m)
            in_z(j, 1, chunk, fs).wait_recv()
            in_y(j, chunk, grp).start()

        loop(0, (n - 1) * m, body)

    def in_from_y(j):
        def body(i):
            s = lax.rem(sp + 1 + i // m, n)
            in_y(j, s * m + lax.rem(fs + i, m), 1 - grp).wait_recv()

        loop(0, (n - 1) * m, body)

    def from_z(j):
        def body(d):
            s = lax.rem(sp + d, n)
            chunk = s * m + fs
            arrival(j, chunk).wait_recv()
            loop(1, m, lambda e: along_x(j, s, e, chunk).start())
            along_y(j, chunk, grp).start()

        loop(1, n, body)

    def from_x(j):
        def body(d):
            s = lax.rem(sp + d, n)

            def inner(e):
                chunk = s * m + lax.rem(fs + e, m)
                arrival(j, chunk).wait_recv()
                along_y(j, chunk, grp).start()

            loop(1, m, inner)

        loop(0, n, body)

    def from_y(j):
        loop(
            1,
            chunks,
            lambda d: along_y(j, lax.rem(mine + d, chunks), 1 - grp).wait_recv(),
        )

    def project(i, first, count):
        block = w_in[:, :, pl.ds(first, count)].reshape(chunks * depth, count)
        return jnp.dot(rows[i], block, preferred_element_type=jnp.float32).astype(jnp.bfloat16)

    def tiles(body):
        step = min(TILE, slim)
        for i in range(m):
            loop(0, slim // step, lambda t: body(i, pl.multiple_of(t * step, LANES), step))

    kv_head = fs * heads // per_kv

    def do_keys():
        for i in range(m):
            both = project(i, 0, 2 * kv).astype(jnp.float32)
            picked = []
            for base in (0, kv):
                one = both[:, base : base + HEAD]
                for h in range(1, kv // HEAD):
                    at = base + h * HEAD
                    one = jnp.where(kv_head == h, both[:, at : at + HEAD], one)
                picked.append(one)
            keys[i] = jnp.concatenate(picked, axis=1).astype(jnp.bfloat16)

    def do_query():
        def body(i, at, step):
            query[i, :, pl.ds(at, step)] = project(i, firsts[2] + at, step)

        tiles(body)

    def result(which, f):
        return mine_conv.at[f] if which == 0 else query.at[f, pl.ds(WINDOW, length)]

    def give(which, e):
        full = (conv, attended)[which]
        f = lax.rem(fs + e, m)
        here = pl.ds(pl.multiple_of(fs * slim, LANES), slim)
        return remote(
            result(which, f), full.at[:, here], give_send.at[which, e], give_recv.at[which, fs], {"fs": f}
        )

    def given(which, e):
        full = (conv, attended)[which]
        f = lax.rem(fs + e, m)
        piece = full.at[:, pl.ds(pl.multiple_of(f * slim, LANES), slim)]
        return remote(piece, piece, give_send.at[which, 0], give_recv.at[which, f], to_fs(e))

    def keep(which):
        full = (conv, attended)[which]
        full[:, pl.ds(pl.multiple_of(fs * slim, LANES), slim)] = result(which, fs)[...]

    def do_attention():
        pairs = 2 * HEAD
        blocks = length // WINDOW
        count = heads // 2
        place_q = lax.broadcasted_iota(jnp.int32, (WINDOW, 2 * WINDOW), 0)
        place_k = lax.broadcasted_iota(jnp.int32, (WINDOW, 2 * WINDOW), 1)
        banded = (place_k > place_q) & (place_k <= place_q + WINDOW)
        for i in range(m):

            def body(b):
                row = pl.multiple_of(b * WINDOW, WINDOW)
                band = keys[i, pl.ds(row, 2 * WINDOW), :]
                key, value = band[:, :HEAD], band[:, HEAD:]
                least = jnp.where((sp == 0) & (b == 0), WINDOW, 0)
                allowed = banded & (place_k >= least)
                for p in range(count):
                    at = p * pairs
                    both = query[i, pl.ds(row + WINDOW, WINDOW), pl.ds(at, pairs)]
                    results = []
                    for half in range(2):
                        one = both[:, half * HEAD : (half + 1) * HEAD]
                        scores = lax.dot_general(
                            one, key, (((1,), (1,)), ((), ())), preferred_element_type=jnp.float32
                        ) * (1.0 / HEAD**0.5)
                        scores = jnp.where(allowed, scores, -jnp.inf)
                        logit = sink[fs * heads + 2 * p + half]
                        peak = jnp.maximum(jnp.max(scores, axis=-1, keepdims=True), logit)
                        powers = jnp.exp(scores - peak)
                        norm = jnp.sum(powers, axis=-1, keepdims=True) + jnp.exp(logit - peak)
                        probs = (powers / norm).astype(jnp.bfloat16)
                        results.append(jnp.dot(probs, value, preferred_element_type=jnp.float32))
                    query[i, pl.ds(row + WINDOW, WINDOW), pl.ds(at, pairs)] = jnp.concatenate(
                        results, axis=1
                    ).astype(jnp.bfloat16)

            loop(0, blocks, body)

    def do_gate():
        def body(i, at, step):
            gate[i, :, pl.ds(at, step)] = project(i, firsts[3] + at, step)

        tiles(body)

    def do_gated():
        def body(i, at, step):
            values = project(i, firsts[4] + at, step)
            product = gate[i, :, pl.ds(at, step)].astype(jnp.float32) * values.astype(jnp.float32)
            gate[i, :, pl.ds(at, step)] = product.astype(jnp.bfloat16)

        tiles(body)

    def do_conv():
        def body(i, at, step):
            outer = project(i, firsts[5] + at, step)[WINDOW:].astype(jnp.float32)
            mixed = None
            gated = gate[i, pl.ds(WINDOW - HALO, HALO + length), pl.ds(at, step)].astype(jnp.float32)
            for which in range(TAPS):
                there = pl.multiple_of(fs * slim + at, LANES)
                tap = taps[pl.ds(which, 1), pl.ds(there, step)].astype(jnp.float32)
                low = HALO - TAPS + 1 + which
                term = tap * gated[low : low + length]
                mixed = term if mixed is None else mixed + term
            mine_conv[i, :, pl.ds(at, step)] = (outer * mixed).astype(jnp.bfloat16)

        tiles(body)

    per = max(1, LANES // across_out)
    step_out = per * across_out
    turns = chunks // per

    def term(which, left, low, count, t):
        block = jnp.concatenate([w_out[which, t * per + i] for i in range(per)], axis=1)
        return jnp.dot(left[pl.ds(low, count), :], block, preferred_element_type=jnp.float32)

    def piece_of(t):
        return pl.ds(pl.multiple_of(t * step_out, LANES), step_out)

    def do_first():
        def body(t):
            total[:, piece_of(t)] = term(0, conv, 0, length, t)

        loop(0, turns, body)

    def swap(t):
        return remote(
            partial.at[:, piece_of(t)],
            theirs.at[:, piece_of(t)],
            swap_send.at[t],
            swap_recv.at[t],
            other_core,
        )

    def work(j):
        if j == 1:
            do_keys()
        if j == 2:
            do_query()
            do_attention()
        if j == 3:
            loop(1, m, lambda e: give(1, e).start())
            keep(1)
            do_gate()
        if j == 4:
            do_gated()
        if j == 5:
            do_conv()

    for step in range(10):
        if step < 6:
            in_from_z(step)
        elif step < 8:
            from_z(step - 6)
        if 7 <= step < 9:
            from_x(step - 7)
        if 2 <= step < 8:
            in_from_y(step - 2)
            work(step - 2)
        if step == 8:
            loop(1, m, lambda e: give(0, e).start())
            keep(0)
            from_y(0)
            loop(1, m, lambda e: given(0, e).wait_recv())
            do_first()
            loop(1, m, lambda e: given(1, e).wait_recv())
        if step == 9:
            from_y(1)

    low_mine = pl.multiple_of(tp * own, LANES)
    low_other = pl.multiple_of((1 - tp) * own, LANES)

    def final(t):
        partial[:, piece_of(t)] = (
            total[pl.ds(low_other, own), piece_of(t)] + term(1, attended, low_other, own, t)
        ).astype(jnp.bfloat16)
        total[pl.ds(low_mine, own), piece_of(t)] = (
            (total[pl.ds(low_mine, own), piece_of(t)] + term(1, attended, low_mine, own, t))
            .astype(jnp.bfloat16)
            .astype(jnp.float32)
        )
        swap(t).start()

    loop(0, turns, final)

    def add(t):
        swap(t).wait()
        out[:, piece_of(t)] = (
            total[pl.ds(low_mine, own), piece_of(t)] + theirs[:, piece_of(t)].astype(jnp.float32)
        ).astype(jnp.bfloat16)

    loop(0, turns, add)

    for j in range(6):
        loop(1, m, lambda e: trade(j, e).wait_send())
        for f in range(m):
            loop(1, n, lambda d: in_z(j, d, sp * m + f, f).wait_send())

        def in_y_done(i):
            s = lax.rem(sp + 1 + i // m, n)
            in_y(j, s * m + lax.rem(fs + i, m), grp).wait_send()

        loop(0, (n - 1) * m, in_y_done)
    for j in range(2):
        loop(1, n, lambda d: along_z(j, d).wait_send())

        def x_done(d):
            s = lax.rem(sp + d, n)
            loop(1, m, lambda e: along_x(j, s, e, s * m + fs).wait_send())

        loop(0, n, x_done)
        loop(1, chunks, lambda d: along_y(j, lax.rem(mine + d, chunks), grp).wait_send())
        loop(1, m, lambda e: give(j, e).wait_send())
    loop(1, m, lambda e: rows_x(e).wait_send())
    loop(0, m, lambda f: rows_core(f).wait_send())

    @pl.when((tp == 1) & (sp < n - 1))
    def _():
        onward.wait_send()

    @pl.when((tp == 1) & (sp > 0))
    def _():
        loop(1, m, lambda e: halo_copy(halo_here(fs), fs, m + e, to_fs(e)).wait_send())
        loop(0, m, lambda f: halo_copy(halo_here(f), f, 1 + f, other_core).wait_send())


def local(
    n,
    m,
    tokens,
    norm_gain,
    w_bgate,
    w_cgate,
    w_conv_in,
    conv_taps,
    w_query,
    w_key,
    w_value,
    sink_logits,
    conv_out_weight,
    attn_out_weight,
):
    widened = tokens[0].astype(jnp.float32)
    normed = (
        widened
        * lax.rsqrt(jnp.mean(widened * widened, axis=-1, keepdims=True) + epsilon)
        * norm_gain
    ).astype(jnp.bfloat16)
    own, features = normed.shape
    span = WINDOW + 2 * own
    depth, kv = w_key.shape
    width = w_query.shape[1]
    slim = width // m
    chunks = n * m
    bf16 = jnp.bfloat16
    vmem = pl.BlockSpec(memory_space=pltpu.VMEM)
    dma = pltpu.SemaphoreType.DMA
    mixed = pl.pallas_call(
        functools.partial(kernel, n, m),
        out_shape=jax.ShapeDtypeStruct((own, features), bf16),
        in_specs=[vmem] * 10 + [pl.BlockSpec(memory_space=pltpu.SMEM)],
        out_specs=vmem,
        scratch_shapes=[
            pltpu.VMEM((chunks, depth, 2 * kv + 4 * slim), bf16),
            pltpu.VMEM((2, chunks) + conv_out_weight.shape, bf16),
            pltpu.VMEM((m, span, features), bf16),
            pltpu.VMEM((m, span, slim), bf16),
            pltpu.VMEM((m, span, 2 * HEAD), bf16),
            pltpu.VMEM((m, span, slim), bf16),
            pltpu.VMEM((m, 2 * own, slim), bf16),
            pltpu.VMEM((2 * own, width), bf16),
            pltpu.VMEM((2 * own, width), bf16),
            pltpu.VMEM((2 * own, features), jnp.float32),
            pltpu.VMEM((own, features), bf16),
            pltpu.VMEM((own, features), bf16),
            dma((9,)),
            dma((2 * m,)),
            dma((m, 2)),
            dma((2 * m,)),
            dma((m,)),
            dma((6, m)),
            dma((6, m)),
            dma((6, n, m)),
            dma((6, chunks)),
            dma((6, chunks)),
            dma((6, chunks)),
            dma((2, n)),
            dma((2, n, m)),
            dma((2, chunks)),
            dma((2, chunks)),
            dma((2, chunks)),
            dma((2, m)),
            dma((2, m)),
            dma((chunks,)),
            dma((chunks,)),
        ],
        compiler_params=pltpu.CompilerParams(
            collective_id=0, has_side_effects=True, vmem_limit_bytes=67_000_000
        ),
    )(
        normed,
        w_key,
        w_value,
        w_query,
        w_cgate,
        w_conv_in,
        w_bgate,
        conv_out_weight,
        attn_out_weight,
        conv_taps,
        sink_logits,
    )
    return mixed[None]


def solution(mesh):
    placed = (
        P(("grp", "fs"), ("sp", "tp"), None),
        P(),
        P(("sp", "fs"), "tp"),
        P(("sp", "fs"), "tp"),
        P(("sp", "fs"), "tp"),
        P(None, "tp"),
        P(("sp", "fs"), "tp"),
        P(("sp", "fs"), "tp"),
        P(("sp", "fs"), "tp"),
        P("tp"),
        P("tp", ("sp", "fs")),
        P("tp", ("sp", "fs")),
    )
    return jax.shard_map(
        functools.partial(local, mesh.shape["sp"], mesh.shape["fs"]),
        mesh=mesh,
        in_specs=placed,
        out_specs=P(("grp", "fs"), ("sp", "tp"), None),
        check_vma=False,
    )
```

time: 435 us -> 268 us (0.62)
  Pallas kernels: 0 us -> 260 us
  waiting for transfers between devices: 220 us -> 0 us
  blocking collectives: 79.7 us -> 0 us
  matrix products: 44.6 us -> 0 us
  starting transfers between devices: 37.6 us -> 0 us
  local copies, waits for them, and re-layouts: 23.4 us -> 2.31 us
  between operations: 13.9 us -> 0.02 us
  other arithmetic: 13.3 us -> 3.58 us
    pallas_call x0 -> x1, Pallas kernels: none -> 260 us  [local(): pl.pallas_call(functools.partial(kernel, n, m), out_shape=jax.ShapeDtypeS...]
    all_gather x7 -> x0, waiting for transfers between devices: 198 us -> none  [the longest x1 67.3 us: local(): lax.all_gather(attn_out_weight, ('sp', 'fs'), axis=1, tiled=True)]
    all_to_all x4 -> x0, blocking collectives: 50.7 us -> none  [the longest x1 16.1 us: local(): lax.all_to_all(in_weights[1], 'fs', split_axis=1, concat_axis=0, tiled=True)]
    dot_general x10 -> x0, matrix products: 44.6 us -> none  [the longest x6 25.9 us: project_all(): jnp.dot(features, weight, preferred_element_type=jnp.float32)]
    all_gather x2 -> x0, blocking collectives: 29 us -> none  [the longest x1 14.8 us: local(): lax.all_gather(narrowed[5], 'sp', axis=0, tiled=True)]
    all_to_all x8 -> x0, starting transfers between devices: 28.8 us -> none  [the longest x6 22.2 us: local(): lax.all_to_all(shortened(rounded), 'fs', split_axis=0, concat_axis=1, til...]
    reduce_scatter x1 -> x0, waiting for transfers between devices: 11.4 us -> none  [local(): lax.psum_scatter((product + jnp.dot(attended, out_columns[1], preferred_e...]
    all_to_all x12 -> x0, local copies, waits for them, and re-layouts: 10.8 us -> none  [the longest x6 6.7 us: local(): lax.all_to_all(shortened(rounded), 'fs', split_axis=0, concat_axis=1, til...]
  transfers between devices with their start and end apart: 19 -> 0, of which waited for: 9 -> 0; matrix products, arithmetic and copies ran while one was open for 16% -> 0% of each run, Pallas kernels for 0% -> 0%
where the time goes in v2:
time: 268 us; the launch traced here: 266 us
  Pallas kernels  260 us (97%)
  other arithmetic  3.58 us (1%)
    pallas_call x1, Pallas kernels, local(): pl.pallas_call(functools.partial(kernel, n, m), out_shape=jax.ShapeDtypeS...  260 us

profile of v2, /device:TPU:9, one launch (start us, length us, event | category | flops | bytes accessed | tf_op | source)
XLA Modules:
  0.0 266.2 jit_solution(12878071364784653005)
XLA Ops:
  0.0 0.0 copy-start
  0.0 1.6 fusion
  1.6 0.0 copy-done
  1.6 2.0 fusion.2.normed
  3.6 260.2 %shard_map.118 = bf16[256,2048]{1,0:T(8,128)(2,1)} custom-call(bf16[256,2048]{1,0:T(8,128)(2,1)} %fusion.2.normed, bf16[256,128]{1,0:T(8,128)(2,1)} %w_key.1, bf16[256,128]{1,0:T(8,128)(2,1)} %w_value.1, bf16[256,1024]{1,0:T(8,128)(2,1)} %w_query.1, bf16[256,1024]{1,0:T(8,128)(2,1)} %w_cgate.1, bf16[256,1024]{1,0:T(8,128)(2,1)} %w_conv_in.1, ...), custom_call_target="tpu_custom_call" | custom-call | tf_op jit(solution)/shard_map/pallas_call | solution.py:598
  263.9 2.3 copy.14
  (1 shorter events, 0.0 us)
Async XLA Ops:
  0.0 1.6 copy-start

commit v3 on v2

--- a/solution.py
+++ b/solution.py
@@ -19,8 +19,8 @@
 epsilon = 1e-06
 
 
-def part(count, eighths):
-    return max(UNIT, count * eighths // 8 // UNIT * UNIT)
+def part(count, sixteenths):
+    return max(UNIT, count * sixteenths // 16 // UNIT * UNIT)
 
 
 def kernel(
@@ -59,9 +59,11 @@
     trade_recv,
     in_send,
     in_recv,
+    in_on,
     in_y_send,
     in_y_recv,
     z_send,
+    z_on,
     x_send,
     out_recv,
     y_send,
@@ -85,8 +87,8 @@
     chunks = n * m
     firsts = [0, kv] + [2 * kv + i * slim for i in range(4)]
     sizes = [kv, kv] + [slim] * 4
-    in_alone = [part(depth, 4)] * 6
-    out_alone = [part(width, 4), part(width, 3)]
+    in_alone = [part(depth, 7)] * 6
+    out_alone = [part(width, 7), part(width, 5)]
 
     grp, sp = lax.axis_index("grp"), lax.axis_index("sp")
     fs, tp = lax.axis_index("fs"), lax.axis_index("tp")
@@ -175,9 +177,37 @@
             pl.multiple_of(group * (depth - in_alone[j]), UNIT), in_alone[j]
         )
 
-    def in_z(j, d, chunk, f):
+    steps = (1, -1, 2, -2)
+
+    def near(body):
+        for slot, by in enumerate(steps):
+            there = sp + by
+
+            @pl.when((there >= 0) & (there < n))
+            def _():
+                body(slot, jnp.clip(there, 0, n - 1))
+
+    def hand_on(s, body):
+        @pl.when((sp - s >= 2) & (sp < n - 1))
+        def _():
+            body(jnp.minimum(sp + 1, n - 1))
+
+        @pl.when((s - sp >= 2) & (sp > 0))
+        def _():
+            body(jnp.maximum(sp - 1, 0))
+
+    def other_sp(d):
+        return lax.rem(jnp.where(2 * sp >= n, sp - d + n, sp + d), n)
+
+    def in_z(j, slot, chunk, f, there):
         piece = w_in.at[chunk, in_rows(j), kept(j)]
-        return remote(piece, piece, in_send.at[j, d, f], in_recv.at[j, chunk], to_sp(d))
+        return remote(
+            piece, piece, in_send.at[j, slot, f], in_recv.at[j, chunk], {"sp": there}
+        )
+
+    def in_hand(j, chunk, there):
+        piece = w_in.at[chunk, in_rows(j), kept(j)]
+        return remote(piece, piece, in_on.at[j, chunk], in_recv.at[j, chunk], {"sp": there})
 
     def in_y(j, chunk, group):
         piece = w_in.at[chunk, in_lone(j, group), kept(j)]
@@ -211,9 +241,13 @@
     def out_lone(j, group):
         return pl.ds(pl.multiple_of(group * (width - out_alone[j]), UNIT), out_alone[j])
 
-    def along_z(j, d):
+    def along_z(j, slot, there):
         piece = w_out.at[j, mine, out_rows(j)]
-        return remote(piece, piece, z_send.at[j, d], out_recv.at[j, mine], to_sp(d))
+        return remote(piece, piece, z_send.at[j, slot], out_recv.at[j, mine], {"sp": there})
+
+    def out_hand(j, chunk, there):
+        piece = w_out.at[j, chunk, out_rows(j)]
+        return remote(piece, piece, z_on.at[j, chunk], out_recv.at[j, chunk], {"sp": there})
 
     def along_x(j, s, e, chunk):
         piece = w_out.at[j, chunk, out_rows(j)]
@@ -227,32 +261,46 @@
         piece = w_out.at[j, chunk, out_lone(j, group)]
         return remote(piece, piece, y_send.at[j, chunk], y_recv.at[j, chunk], other_grp)
 
-    for j in range(6):
-        loop(1, m, lambda e: trade(j, e).start())
-        if j == 1:
-
-            @pl.when((tp == 1) & (sp < n - 1))
-            def _():
-                onward.start()
-
-    loop(1, m, lambda e: rows_x(e).start())
-    for j in range(6):
+    def own_in(j):
         fills[j].wait()
-        loop(1, n, lambda d: in_z(j, d, mine, fs).start())
-    fills[8].wait()
-    rows_core(fs).start()
-    for j in range(6):
-
+        near(lambda slot, there: in_z(j, slot, mine, fs, there).start())
+
+    def traded_in(j):
         def traded(e):
             f = lax.rem(fs + e, m)
             trade_arrival(j, f).wait_recv()
-            loop(1, n, lambda d: in_z(j, d, sp * m + f, f).start())
+            near(lambda slot, there: in_z(j, slot, sp * m + f, f, there).start())
 
         loop(1, m, traded)
-    for j in range(2):
+
+    def own_out(j):
         fills[6 + j].wait()
-        loop(1, n, lambda d: along_z(j, d).start())
+        near(lambda slot, there: along_z(j, slot, there).start())
         loop(1, m, lambda e: along_x(j, sp, e, mine).start())
+
+    for j in range(3):
+        loop(1, m, lambda e: trade(j, e).start())
+        own_in(j)
+
+    @pl.when((tp == 1) & (sp < n - 1))
+    def _():
+        onward.start()
+
+    loop(1, m, lambda e: rows_x(e).start())
+    for j in range(3, 6):
+        loop(1, m, lambda e: trade(j, e).start())
+    fills[8].wait()
+    rows_core(fs).start()
+    for j in range(3):
+        traded_in(j)
+    own_in(3)
+    own_out(0)
+    own_in(4)
+    traded_in(3)
+    own_in(5)
+    traded_in(4)
+    traded_in(5)
+    own_out(1)
 
     def rows_on(e):
         f = lax.rem(fs + e, m)
@@ -286,25 +334,27 @@
 
     def in_from_z(j):
         def body(i):
-            s = lax.rem(sp + 1 + i // m, n)
+            s = other_sp(1 + i // m)
             chunk = s * m + lax.rem(fs + i, m)
-            in_z(j, 1, chunk, fs).wait_recv()
+            in_hand(j, chunk, sp).wait_recv()
+            hand_on(s, lambda there: in_hand(j, chunk, there).start())
             in_y(j, chunk, grp).start()
 
         loop(0, (n - 1) * m, body)
 
     def in_from_y(j):
         def body(i):
-            s = lax.rem(sp + 1 + i // m, n)
+            s = other_sp(1 + i // m)
             in_y(j, s * m + lax.rem(fs + i, m), 1 - grp).wait_recv()
 
         loop(0, (n - 1) * m, body)
 
     def from_z(j):
         def body(d):
-            s = lax.rem(sp + d, n)
+            s = other_sp(d)
             chunk = s * m + fs
             arrival(j, chunk).wait_recv()
+            hand_on(s, lambda there: out_hand(j, chunk, there).start())
             loop(1, m, lambda e: along_x(j, s, e, chunk).start())
             along_y(j, chunk, grp).start()
 
@@ -487,25 +537,28 @@
         if j == 5:
             do_conv()
 
+    order = (0, 1, 2, 3, 6, 4, 5, 7)
     for step in range(10):
-        if step < 6:
-            in_from_z(step)
-        elif step < 8:
-            from_z(step - 6)
-        if 7 <= step < 9:
-            from_x(step - 7)
-        if 2 <= step < 8:
-            in_from_y(step - 2)
-            work(step - 2)
+        if step < 8:
+            item = order[step]
+            in_from_z(item) if item < 6 else from_z(item - 6)
+        if 1 <= step < 9 and order[step - 1] >= 6:
+            from_x(order[step - 1] - 6)
+        if step >= 2:
+            item = order[step - 2]
+            if item < 6:
+                in_from_y(item)
+                work(item)
+            elif item == 6:
+                from_y(0)
+            else:
+                loop(1, m, lambda e: given(0, e).wait_recv())
+                do_first()
+                loop(1, m, lambda e: given(1, e).wait_recv())
+                from_y(1)
         if step == 8:
             loop(1, m, lambda e: give(0, e).start())
             keep(0)
-            from_y(0)
-            loop(1, m, lambda e: given(0, e).wait_recv())
-            do_first()
-            loop(1, m, lambda e: given(1, e).wait_recv())
-        if step == 9:
-            from_y(1)
 
     low_mine = pl.multiple_of(tp * own, LANES)
     low_other = pl.multiple_of((1 - tp) * own, LANES)
@@ -534,18 +587,21 @@
     for j in range(6):
         loop(1, m, lambda e: trade(j, e).wait_send())
         for f in range(m):
-            loop(1, n, lambda d: in_z(j, d, sp * m + f, f).wait_send())
+            near(lambda slot, there: in_z(j, slot, sp * m + f, f, there).wait_send())
 
         def in_y_done(i):
-            s = lax.rem(sp + 1 + i // m, n)
-            in_y(j, s * m + lax.rem(fs + i, m), grp).wait_send()
+            s = other_sp(1 + i // m)
+            chunk = s * m + lax.rem(fs + i, m)
+            in_y(j, chunk, grp).wait_send()
+            hand_on(s, lambda there: in_hand(j, chunk, there).wait_send())
 
         loop(0, (n - 1) * m, in_y_done)
     for j in range(2):
-        loop(1, n, lambda d: along_z(j, d).wait_send())
+        near(lambda slot, there: along_z(j, slot, there).wait_send())
 
         def x_done(d):
             s = lax.rem(sp + d, n)
+            hand_on(s, lambda there: out_hand(j, s * m + fs, there).wait_send())
             loop(1, m, lambda e: along_x(j, s, e, s * m + fs).wait_send())
 
         loop(0, n, x_done)
@@ -620,11 +676,13 @@
             dma((m,)),
             dma((6, m)),
             dma((6, m)),
-            dma((6, n, m)),
+            dma((6, 4, m)),
             dma((6, chunks)),
             dma((6, chunks)),
             dma((6, chunks)),
-            dma((2, n)),
+            dma((6, chunks)),
+            dma((2, 4)),
+            dma((2, chunks)),
             dma((2, n, m)),
             dma((2, chunks)),
             dma((2, chunks)),

time: 268 us -> 230 us (0.86)
  the two profiles are of different devices: /device:TPU:9 before, /device:TPU:3 now
where the time goes in v3:
time: 230 us
  Pallas kernels  224 us (97%)
  other arithmetic  3.58 us (2%)
  local copies, waits for them, and re-layouts  2.31 us (1%)
    pallas_call x1, Pallas kernels, local(): pl.pallas_call(functools.partial(kernel, n, m), out_shape=jax.ShapeDtypeS...  224 us

profile of v3, /device:TPU:3, one launch (start us, length us, event | category | flops | bytes accessed | tf_op | source)
XLA Modules:
  0.0 229.8 jit_solution(2366558787689978350)
XLA Ops:
  0.0 0.0 copy-start
  0.0 1.6 fusion
  1.6 0.0 copy-done
  1.6 2.0 fusion.2.normed
  3.6 223.9 %shard_map.118 = bf16[256,2048]{1,0:T(8,128)(2,1)} custom-call(bf16[256,2048]{1,0:T(8,128)(2,1)} %fusion.2.normed, bf16[256,128]{1,0:T(8,128)(2,1)} %w_key.1, bf16[256,128]{1,0:T(8,128)(2,1)} %w_value.1, bf16[256,1024]{1,0:T(8,128)(2,1)} %w_query.1, bf16[256,1024]{1,0:T(8,128)(2,1)} %w_cgate.1, bf16[256,1024]{1,0:T(8,128)(2,1)} %w_conv_in.1, ...), custom_call_target="tpu_custom_call" | custom-call | tf_op jit(solution)/shard_map/pallas_call | solution.py:654
  227.5 2.3 %copy.14 = bf16[1,256,2048]{2,1,0:T(8,128)(2,1)} copy(bf16[1,256,2048]{2,1,0:T(8,128)(2,1)} %bitcast.5) | data formatting | bytes 2097152
  (1 shorter events, 0.0 us)
Async XLA Ops:
  0.0 1.6 copy-start
